TPU v7x, 512 devices: a whole 4x4x16 slice. The times are simulated.
512 devices in a mesh: sp: 64 (over z, y), tp: 8 (over x, core).
Axes of the slice: x: 4, y: 4, z: 16, core: 2. Of those that a mesh axis runs over, the one named last changes fastest.
Arguments:
- latent: bfloat16 [49152, 2048], P(('sp', 'tp')), may hold values from -6 to 6
- condition: float32 [2048], P('sp'), may hold values from -6 to 6
- context_condition: float32 [2048], P('sp'), may hold values from -6 to 6
- context: bfloat16 [1024, 2048], P('sp'), may hold values from -6 to 6
- norm_gain: float32 [2048], replicated, may hold values from 0.1 to 1.9
- shift_weight: bfloat16 [2048, 2048], P('sp', 'tp'), may hold values from -0.375 to 0.375
- scale_weight: bfloat16 [2048, 2048], P('sp', 'tp'), may hold values from -0.375 to 0.375
- gate_weight: bfloat16 [2048, 2048], P('sp', 'tp'), may hold values from -0.375 to 0.375
- query_weight: bfloat16 [2048, 2048], P(None, 'tp'), may hold values from -2 to 2
- key_matrix: bfloat16 [2048, 1024], P(None, 'tp'), may hold values from -2 to 2
- value_matrix: bfloat16 [2048, 1024], P(None, 'tp'), may hold values from -0.125 to 0.125
- sink_logit_head: float32 [16], P('tp'), may hold values from 6 to 10
- out_weight: bfloat16 [2048, 2048], P('tp'), may hold values from -0.125 to 0.125
Outputs:
- updated: bfloat16 [49152, 2048], P(('sp', 'tp'))
All inputs are finite; a program needn't handle non-finite values.
Results may differ from a plain program's by a relative error of at most 0.012.
The roundings to bfloat16 on the way count: a program that leaves them out, or rounds other values in their place, can miss the bound.
Values may be sent and summed in bfloat16 or wider, within the bound.
A program may use at most 64 MiB of HBM per device.

v0:
```python
import functools
import jax
import jax.numpy as jnp
from jax import lax
from jax.sharding import Mesh
from jax.sharding import PartitionSpec as P

QUERY_HEADS = 16
KEY_VALUE_HEADS = 8
HEAD_DIM = 128
WINDOW_REACH = 128
GRID_W = 64
SP = ("sp_0", "sp_1")
SP_TP = ("sp_0", "sp_1", "tp")
NORM_EPS = 1e-05
MASKED_SCORE = -1e30


def one_axis_at_a_time(x, axes):
    return functools.reduce(lax.psum, axes, x)


def side_by_side(arrays, axis, dim, along):
    both = jnp.concatenate(arrays, axis=along)
    out, at, outs = (lax.all_gather(both, axis, axis=dim, tiled=True), 0, [])
    for a in arrays:
        outs.append(lax.slice_in_dim(out, at, at + a.shape[along], axis=along))
        at += a.shape[along]
    return tuple(outs)


def padded_2(block, sides, width):
    for axis, dim in sides:
        count = lax.axis_size(axis)
        forward = [(i, i + 1) for i in range(count - 1)]
        backward = [(target, source) for source, target in forward]
        low = lax.ppermute(
            lax.slice_in_dim(block, block.shape[dim] - width, None, axis=dim), axis, forward
        )
        high = lax.ppermute(lax.slice_in_dim(block, 0, width, axis=dim), axis, backward)
        block = jnp.concatenate([low, block, high], axis=dim)
    return block


def sent_to_all(x, axis):
    peers = lax.axis_size(axis)
    return lax.all_to_all(jnp.broadcast_to(x[None], (peers, *x.shape)), axis, 0, 0, tiled=True)


def laid_out(blocks, dim):
    blocks = jnp.moveaxis(blocks, 0, dim)
    shape = blocks.shape
    return blocks.reshape(*shape[:dim], shape[dim] * shape[dim + 1], *shape[dim + 2 :])


def gathered_copies(x, axis, dim):
    blocks = sent_to_all(x, axis)
    return laid_out(blocks, dim)


def in_blocks(x, dim, peers):
    before, after = (x.shape[:dim], x.shape[dim + 1 :])
    return jnp.moveaxis(x.reshape(*before, peers, -1, *after), dim, 0)


def summed_on_arrival(x, axis, dim):
    peers = lax.axis_size(axis)
    blocks = lax.all_to_all(in_blocks(x, dim, peers), axis, 0, 0, tiled=True)
    return jnp.sum(blocks.astype(jnp.float32), axis=0)


def rotate(vectors, position):
    quarter = HEAD_DIM // 4
    grid_row = (position // GRID_W).astype(jnp.float32)
    grid_col = (position % GRID_W).astype(jnp.float32)
    inv_freq = 10000.0 ** (-jnp.arange(0, HEAD_DIM // 2, 2, dtype=jnp.float32) / (HEAD_DIM // 2))
    angles = jnp.concatenate([grid_row[:, None] * inv_freq, grid_col[:, None] * inv_freq], axis=-1)
    cosine_table = jnp.cos(angles).reshape(-1, 1, 2, quarter)
    sine_table = jnp.sin(angles).reshape(-1, 1, 2, quarter)
    pieces = vectors.reshape(vectors.shape[0], vectors.shape[1], 2, 2, quarter)
    first_half = pieces[..., 0, :]
    second_half = pieces[..., 1, :]
    turned = jnp.stack(
        [
            first_half * cosine_table - second_half * sine_table,
            first_half * sine_table + second_half * cosine_table,
        ],
        axis=-2,
    )
    return turned.reshape(vectors.shape)


def modulated_norm(rows_in, norm_gain, shift, scale):
    floats = rows_in.astype(jnp.float32)
    normed = (
        floats * lax.rsqrt(jnp.mean(floats * floats, axis=-1, keepdims=True) + NORM_EPS) * norm_gain
    )
    return (normed * (1.0 + scale) + shift).astype(jnp.bfloat16)


def shards(
    latent,
    condition,
    context_condition,
    context,
    norm_gain,
    shift_weight,
    scale_weight,
    gate_weight,
    query_weight,
    key_matrix,
    value_matrix,
    sink_logit_head,
    out_weight,
):
    tp_count = lax.axis_size("tp")
    group_rows = latent.shape[0] * tp_count
    offset = lax.axis_index(SP) * group_rows
    total_rows = group_rows * lax.axis_size(SP)
    active = jax.nn.silu(jnp.stack([condition, context_condition])).astype(jnp.bfloat16)
    shift_part = jnp.dot(active, shift_weight, preferred_element_type=jnp.float32)
    scale_part = jnp.dot(active, scale_weight, preferred_element_type=jnp.float32)
    gate_part = jnp.dot(active[:1], gate_weight, preferred_element_type=jnp.float32)
    shift_sum, scale_sum, gate_sum = (
        one_axis_at_a_time(shift_part, SP),
        one_axis_at_a_time(scale_part, SP),
        one_axis_at_a_time(gate_part, SP),
    )
    shift_all, scale_all, gate_all = side_by_side((shift_sum, scale_sum, gate_sum), "tp", 1, 0)
    hidden_state = modulated_norm(latent, norm_gain, shift_all[0], scale_all[0])
    query_width = query_weight.shape[1]
    pair_width = key_matrix.shape[1]
    block_rows = lax.all_gather(hidden_state, "tp", axis=0, tiled=True)
    row_count = block_rows.shape[0]
    position = offset + jnp.arange(row_count, dtype=jnp.int32)
    query_row_block = jnp.dot(block_rows, query_weight, preferred_element_type=jnp.float32)
    query_row_block = rotate(query_row_block.reshape(row_count, -1, HEAD_DIM), position)
    key_rows = jnp.dot(block_rows, key_matrix, preferred_element_type=jnp.float32)
    key_rows = rotate(key_rows.reshape(row_count, -1, HEAD_DIM), position)
    value_rows = jnp.dot(block_rows, value_matrix, preferred_element_type=jnp.float32)
    projected = jnp.concatenate(
        [
            query_row_block.reshape(row_count, query_width),
            key_rows.reshape(row_count, pair_width),
            value_rows,
        ],
        axis=1,
    ).astype(jnp.bfloat16)
    padded = padded_2(projected[:, query_width:], ((SP, 0),), WINDOW_REACH)
    ctx_hidden = modulated_norm(context, norm_gain, shift_all[1], scale_all[1])
    ctx_pairs = gathered_copies(
        jnp.concatenate(
            [
                jnp.dot(ctx_hidden, key_matrix, preferred_element_type=jnp.float32),
                jnp.dot(ctx_hidden, value_matrix, preferred_element_type=jnp.float32),
            ],
            axis=1,
        ).astype(jnp.bfloat16),
        SP,
        0,
    )
    blocks = group_rows // WINDOW_REACH
    kv_local = pair_width // HEAD_DIM
    queries_per_group = QUERY_HEADS // KEY_VALUE_HEADS
    query_blocks = projected[:, :query_width].reshape(
        blocks, WINDOW_REACH, kv_local, queries_per_group, HEAD_DIM
    )
    key_pad = padded[:, :pair_width].reshape(blocks + 2, WINDOW_REACH, kv_local, HEAD_DIM)
    value_pad = padded[:, pair_width:].reshape(blocks + 2, WINDOW_REACH, kv_local, HEAD_DIM)
    band_keys = jnp.concatenate([key_pad[:-2], key_pad[1:-1], key_pad[2:]], axis=1)
    band_values = jnp.concatenate([value_pad[:-2], value_pad[1:-1], value_pad[2:]], axis=1)
    context_key_rows = ctx_pairs[:, :pair_width].reshape(-1, kv_local, HEAD_DIM)
    context_value_rows = ctx_pairs[:, pair_width:].reshape(-1, kv_local, HEAD_DIM)
    factor = HEAD_DIM ** (-0.5)
    band_scores = (
        jnp.einsum("nqhgd,nkhd->nhgqk", query_blocks, band_keys, preferred_element_type=jnp.float32)
        * factor
    )
    block_ids = jnp.arange(blocks, dtype=jnp.int32)[:, None, None]
    query_pos = (
        offset + block_ids * WINDOW_REACH + jnp.arange(WINDOW_REACH, dtype=jnp.int32)[None, :, None]
    )
    key_pos = (
        offset
        + (block_ids - 1) * WINDOW_REACH
        + jnp.arange(3 * WINDOW_REACH, dtype=jnp.int32)[None, None, :]
    )
    allowed = (
        (jnp.abs(key_pos - query_pos) <= WINDOW_REACH) & (key_pos >= 0) & (key_pos < total_rows)
    )
    band_scores = jnp.where(allowed[:, None, None], band_scores, MASKED_SCORE)
    ctx_scores = (
        jnp.einsum(
            "nqhgd,chd->nhgqc", query_blocks, context_key_rows, preferred_element_type=jnp.float32
        )
        * factor
    )
    sink_logit_rows = sink_logit_head.reshape(1, kv_local, queries_per_group, 1, 1)
    maxima = jnp.maximum(
        jnp.maximum(
            jnp.max(band_scores, axis=-1, keepdims=True),
            jnp.max(ctx_scores, axis=-1, keepdims=True),
        ),
        sink_logit_rows,
    )
    band_exp = jnp.exp(band_scores - maxima)
    ctx_exp = jnp.exp(ctx_scores - maxima)
    denominator = (
        jnp.sum(band_exp, axis=-1, keepdims=True)
        + jnp.sum(ctx_exp, axis=-1, keepdims=True)
        + jnp.exp(sink_logit_rows - maxima)
    )
    band_weights = (band_exp / denominator).astype(jnp.bfloat16)
    ctx_weights = (ctx_exp / denominator).astype(jnp.bfloat16)
    attended = jnp.einsum(
        "nhgqk,nkhd->nqhgd", band_weights, band_values, preferred_element_type=jnp.float32
    ) + jnp.einsum(
        "nhgqc,chd->nqhgd", ctx_weights, context_value_rows, preferred_element_type=jnp.float32
    )
    attended = attended.astype(jnp.bfloat16).reshape(group_rows, query_width)
    mixed_sum = summed_on_arrival(
        jnp.dot(attended, out_weight, preferred_element_type=jnp.float32).astype(jnp.bfloat16),
        "tp",
        0,
    )
    return (latent.astype(jnp.float32) + gate_all[0] * mixed_sum).astype(jnp.bfloat16)


def solution(mesh):
    torus = Mesh(mesh.devices.reshape(16, 4, mesh.shape["tp"]), ("sp_0", "sp_1", "tp"))
    return jax.shard_map(
        shards,
        mesh=torus,
        in_specs=(
            P(SP_TP, None),
            P(SP),
            P(SP),
            P(SP, None),
            P(),
            P(SP, "tp"),
            P(SP, "tp"),
            P(SP, "tp"),
            P(None, "tp"),
            P(None, "tp"),
            P(None, "tp"),
            P("tp"),
            P("tp", None),
        ),
        out_specs=P(SP_TP, None),
        check_vma=False,
    )
```

profile of v0, /device:TPU:128, one launch (start us, length us, event | category | flops | bytes accessed | tf_op | source)
XLA Modules:
  0.0 187.9 jit_solution(3284651303342493575)
XLA Ops:
  6.6 1.3 fusion.20
  11.1 30.9 %all-reduce = (f32[1,256]{1,0:T(1,128)S(1)}, f32[2,256]{1,0:T(2,128)S(1)}, f32[2,256]{1,0:T(2,128)S(1)}) all-reduce(f32[1,256]{1,0:T(1,128)S(1)} %fusion.59, f32[2,256]{1,0:T(2,128)S(1)} %fusion.71, f32[2,256]{1,0:T(2,128)S(1)} %fusion.70), channel_id=1, replica_groups=mesh['sp_0'=16,'sp_1'=4,'tp'=8] {'sp_0'}, use_global_device_ids=true, to_apply=%region_4.5 | all-reduce | flops 1280 | bytes 10240 | tf_op jit(solution)/shard_map/psum | solution.py:20
  42.0 10.8 %all-reduce.1 = (f32[1,256]{1,0:T(1,128)S(1)}, f32[2,256]{1,0:T(2,128)S(1)}, f32[2,256]{1,0:T(2,128)S(1)}) all-reduce(f32[1,256]{1,0:T(1,128)S(1)} %get-tuple-element.5, f32[2,256]{1,0:T(2,128)S(1)} %get-tuple-element.6, f32[2,256]{1,0:T(2,128)S(1)} %get-tuple-element.7), channel_id=1, replica_groups=mesh['sp_0'=16,'sp_1'=4,'tp'=8] {'sp_1'}, use_global_device_ids=true, to_apply=%region_5.6 | all-reduce | flops 1280 | bytes 10240 | tf_op jit(solution)/shard_map/psum | solution.py:20
  52.9 13.1 %all_gather.6 = f32[5,2048]{1,0:T(8,128)S(1)} all-gather(f32[5,256]{1,0:T(8,128)S(1)} %pad_maximum_fusion.12), channel_id=1, replica_groups=mesh['sp_0'=16,'sp_1'=4,'tp'=8] {'tp'}, dimensions={1}, use_global_device_ids=true | all-gather | bytes 46080 | tf_op jit(solution)/shard_map/all_gather | solution.py:25
  66.0 2.0 %fusion.24 = bf16[96,2048]{1,0:T(8,128)(2,1)} fusion(bf16[96,2048]{1,0:T(8,128)(2,1)} %param.13, f32[2048]{0:T(1024)S(1)} %bitcast.156, f32[2048]{0:T(1024)S(1)} %bitcast.157, f32[2048]{0:T(1024)} %param.17, f32[96]{0:T(128)S(1)} %add_rsqrt_fusion.1), kind=kLoop, calls=%fused_computation.34 | loop fusion | flops 1179648 | bytes 811392 | tf_op jit(solution)/shard_map/convert_element_type | solution.py:98
  68.0 1.0 fusion.42
  69.0 1.3 convolution_convert_fusion.2
  70.6 0.8 broadcast_in_dim.12
  71.5 12.3 %all-to-all-start = ((bf16[64,16,256]{2,1,0:T(8,128)(2,1)}), bf16[64,16,256]{2,1,0:T(8,128)(2,1)S(1)}, u32[]{:S(2)}, u32[]{:S(2)}) async-start(bf16[64,16,256]{2,1,0:T(8,128)(2,1)} %broadcast_in_dim.12), calls=%async_computation | async-start | bytes 1048576 | tf_op jit(solution)/shard_map/all_to_all | solution.py:47
  84.8 1.4 fusion.18
  86.2 14.9 %all-gather.2.cloned.1.call-done = bf16[768,2048]{1,0:T(8,128)(2,1)} async-done(((bf16[96,2048]{1,0:T(8,128)(2,1)}), bf16[768,2048]{1,0:T(8,128)(2,1)}) %all-gather.2.cloned.1.call-update) | async-done | bytes 3145744 | tf_op jit(solution)/shard_map/all_gather | solution.py:133
  101.2 3.0 %fusion.72 = f32[768,128]{0,1:T(8,128)S(1)} fusion(bf16[768,2048]{1,0:T(8,128)(2,1)} %all-gather.2.cloned.1.call-done, bf16[2048,128]{1,0:T(8,128)(2,1)S(1)} %copy-done.3), kind=kOutput, calls=%fused_computation.126 | convolution fusion | flops 402653184 | bytes 4063232 | tf_op jit(solution)/shard_map/dot_general | solution.py:138
  105.2 3.0 %convolution_convert_fusion.1 = bf16[768,128]{1,0:T(8,128)(2,1)S(1)} fusion(bf16[768,2048]{1,0:T(8,128)(2,1)} %all-gather.2.cloned.1.call-done, bf16[2048,128]{1,0:T(8,128)(2,1)S(1)} %copy-done.5), kind=kOutput, calls=%fused_computation.27 | convolution fusion | flops 402751488 | bytes 3866624 | tf_op jit(solution)/shard_map/dot_general | solution.py:140
  108.9 3.4 %collective-permute-start = (bf16[128,256]{1,0:T(8,128)(2,1)}, bf16[128,256]{1,0:T(8,128)(2,1)S(1)}, u32[]{:S(2)}, u32[]{:S(2)}) collective-permute-start(bf16[128,256]{1,0:T(8,128)(2,1)} %get-tuple-element.21), channel_id=1, source_target_pairs={{0,8},{8,16},{16,24},{24,32},{32,40},{40,48},{48,56},{56,64},{64,7... | collective-permute-start | bytes 196616 | tf_op jit(solution)/shard_map/ppermute | solution.py:37
  112.3 5.9 %collective-permute-start.1 = (bf16[128,256]{1,0:T(8,128)(2,1)}, bf16[128,256]{1,0:T(8,128)(2,1)S(1)}, u32[]{:S(2)}, u32[]{:S(2)}) collective-permute-start(bf16[128,256]{1,0:T(8,128)(2,1)} %get-tuple-element.22), channel_id=1, source_target_pairs={{8,0},{16,8},{24,16},{32,24},{40,32},{48,40},{56,48},{64,56},{72,6... | collective-permute-start | bytes 196616 | tf_op jit(solution)/shard_map/ppermute | solution.py:40
  118.3 1.1 fusion.73
  120.3 3.7 %bitcast_reduce_fusion = (f32[6,2,128]{2,1,0:T(2,128)S(1)}, f32[1024,6,128,2]{2,0,3,1:T(8,128)}) fusion(bf16[6,128,2,128]{3,1,2,0:T(8,128)(2,1)S(1)} %copy.27, bf16[1024,256]{1,0:T(8,128)(2,1)S(1)} %bitcast.144), kind=kOutput, calls=%fused_computation.1 | convolution fusion | flops 405797376 | bytes 6952960 | tf_op jit(solution)/shard_map/nqhgd,chd->nhgqc/dot_general | solution.py:193
  126.5 1.5 fusion.6
  128.1 3.8 %fusion.1 = f32[6,2,128]{2,1,0:T(2,128)S(1)} fusion(f32[1024,6,128,2]{2,0,3,1:T(8,128)} %get-tuple-element.41, f32[6,2,128]{2,1,0:T(2,128)S(1)} %maximum_maximum_fusion), kind=kLoop, calls=%fused_computation.5 | loop fusion | flops 4717056 | bytes 6303744 | tf_op jit(solution)/shard_map/reduce_sum | solution.py:210
  134.2 0.9 slice-done.1
  135.1 1.5 fusion.13
  137.0 1.0 convolution_convert_fusion
  138.0 41.2 %all_to_all.10 = bf16[8,96,2048]{2,1,0:T(8,128)(2,1)S(1)} all-to-all(bf16[8,96,2048]{2,1,0:T(8,128)(2,1)S(1)} %bitcast.139), channel_id=1, replica_groups=mesh['sp_0'=16,'sp_1'=4,'tp'=8] {'tp'}, dimensions={0} | all-to-all | bytes 6291456 | tf_op jit(solution)/shard_map/all_to_all | solution.py:68
  180.2 0.8 fusion.25
  (67 shorter events, 13.3 us)
Async XLA Ops:
  6.5 130.5 %copy-start = (bf16[256,2048]{1,0:T(8,128)(2,1)S(1)}, bf16[256,2048]{1,0:T(8,128)(2,1)}, u32[]{:S(2)}) copy-start(bf16[256,2048]{1,0:T(8,128)(2,1)} %param.25) | copy-start | bytes 3145732
  6.5 63.8 %copy-start.7 = (f32[2048]{0:T(1024)S(1)}, f32[2048]{0:T(1024)}, u32[]{:S(2)}) copy-start(f32[2048]{0:T(1024)} %param.17) | copy-start | bytes 24580
  6.5 63.8 %copy-start.4 = (bf16[16,2048]{1,0:T(8,128)(2,1)S(1)}, bf16[16,2048]{1,0:T(8,128)(2,1)}, u32[]{:S(2)}) copy-start(bf16[16,2048]{1,0:T(8,128)(2,1)} %param.16) | copy-start | bytes 196612
  6.5 63.8 %copy-start.3 = (bf16[2048,128]{1,0:T(8,128)(2,1)S(1)}, bf16[2048,128]{1,0:T(8,128)(2,1)}, u32[]{:S(2)}) copy-start(bf16[2048,128]{1,0:T(8,128)(2,1)} %param.22) | copy-start | bytes 1572868
  6.5 94.6 %all-gather.2.cloned.1.call-start = ((), (), s32[]{:S(2)}) async-start(), calls=%async_computation.2 | async-start | bytes 3538944 | tf_op jit(solution)/shard_map/all_gather | solution.py:133
  71.5 48.8 %all-to-all-start = ((bf16[64,16,256]{2,1,0:T(8,128)(2,1)}), bf16[64,16,256]{2,1,0:T(8,128)(2,1)S(1)}, u32[]{:S(2)}, u32[]{:S(2)}) async-start(bf16[64,16,256]{2,1,0:T(8,128)(2,1)} %broadcast_in_dim.12), calls=%async_computation | async-start | bytes 1048576 | tf_op jit(solution)/shard_map/all_to_all | solution.py:47
  86.2 18.9 %copy-start.5 = (bf16[2048,128]{1,0:T(8,128)(2,1)S(1)}, bf16[2048,128]{1,0:T(8,128)(2,1)}, u32[]{:S(2)}) copy-start(bf16[2048,128]{1,0:T(8,128)(2,1)} %param.23) | copy-start | bytes 1572868
  105.2 13.1 %copy-start.2 = (bf16[768,2048]{1,0:T(8,128)(2,1)S(1)}, bf16[768,2048]{1,0:T(8,128)(2,1)}, u32[]{:S(2)}) copy-start(bf16[768,2048]{1,0:T(8,128)(2,1)} %all-gather.2.cloned.1.call-done) | copy-start | bytes 9437188
  105.2 13.1 %copy-start.9 = (bf16[2048,256]{1,0:T(8,128)(2,1)S(1)}, bf16[2048,256]{1,0:T(8,128)(2,1)}, u32[]{:S(2)}) copy-start(bf16[2048,256]{1,0:T(8,128)(2,1)} %param.21) | copy-start | bytes 3145732
  108.9 16.4 %collective-permute-start = (bf16[128,256]{1,0:T(8,128)(2,1)}, bf16[128,256]{1,0:T(8,128)(2,1)S(1)}, u32[]{:S(2)}, u32[]{:S(2)}) collective-permute-start(bf16[128,256]{1,0:T(8,128)(2,1)} %get-tuple-element.21), channel_id=1, source_target_pairs={{0,8},{8,16},{16,24},{24,32},{32,40},{40,48},{48,56},{56,64},{64,7... | collective-permute-start | bytes 196616 | tf_op jit(solution)/shard_map/ppermute | solution.py:37
  112.3 13.0 %collective-permute-start.1 = (bf16[128,256]{1,0:T(8,128)(2,1)}, bf16[128,256]{1,0:T(8,128)(2,1)S(1)}, u32[]{:S(2)}, u32[]{:S(2)}) collective-permute-start(bf16[128,256]{1,0:T(8,128)(2,1)} %get-tuple-element.22), channel_id=1, source_target_pairs={{8,0},{16,8},{24,16},{32,24},{40,32},{48,40},{56,48},{64,56},{72,6... | collective-permute-start | bytes 196616 | tf_op jit(solution)/shard_map/ppermute | solution.py:40
  126.5 1.5 copy-start.8
  131.9 0.9 copy-start.6
  131.9 2.3 %slice-start = ((s8[6291456]{0:T(1024)(128)(4,1)}), s8[4194304]{0:T(1024)(128)(4,1)S(1)}, s32[]{:S(2)}) async-start(s8[6291456]{0:T(1024)(128)(4,1)} %bitcast.137), calls=%async_computation.3 | async-start | bytes 8388608
  132.8 2.2 %slice-start.1 = ((s8[6291456]{0:T(1024)(128)(4,1)}), s8[2097152]{0:T(1024)(128)(4,1)S(1)}, s32[]{:S(2)}) async-start(s8[6291456]{0:T(1024)(128)(4,1)} %bitcast.137), calls=%async_computation.4 | async-start | bytes 4194304
  179.2 1.0 copy-start.1
Sparse Core Ops, SparseCore 0:
  68.2 32.9 all-gather.1
where the time goes:
time: 189 us; the launch traced here: 188 us
  blocking collectives  96.1 us (51%)
  starting transfers between devices  21.6 us (11%)
  matrix products  19.7 us (10%)
  other arithmetic  15.8 us (8%)
  waiting for transfers between devices  15 us (8%)
  between operations  13.8 us (7%)
  local copies, waits for them, and re-layouts  5.96 us (3%)
    psum x2, blocking collectives, one_axis_at_a_time(): return functools.reduce(lax.psum, axes, x)  41.8 us
    all_to_all x1, blocking collectives, summed_on_arrival(): blocks = lax.all_to_all(in_blocks(x, dim, peers), axis, 0, 0, tiled=True)  41.2 us
    all_gather x1, waiting for transfers between devices, shards(): block_rows = lax.all_gather(hidden_state, 'tp', axis=0, tiled=True)  14.9 us
    all_gather x1, blocking collectives, side_by_side(): out, at, outs = (lax.all_gather(both, axis, axis=dim, tiled=True), 0, [])  13.1 us
    all_to_all x1, starting transfers between devices, sent_to_all(): lax.all_to_all(jnp.broadcast_to(x[None], (peers, *x.shape)), axis, 0, 0,...  12.3 us
    ppermute x1, starting transfers between devices, padded_2(): lax.ppermute(lax.slice_in_dim(block, 0, width, axis=dim), axis, backward)  5.93 us
    reduce_sum x1, other arithmetic, shards(): jnp.sum(ctx_exp, axis=-1, keepdims=True)  3.82 us
  transfers between devices with their start and end apart: 4, of which 1 were waited for; matrix products, arithmetic and copies ran while one was open for 11% of the time, Pallas kernels for 0%

commit v1 on v0

--- a/solution.py
+++ b/solution.py
@@ -130,7 +130,8 @@
     hidden_state = modulated_norm(latent, norm_gain, shift_all[0], scale_all[0])
     query_width = query_weight.shape[1]
     pair_width = key_matrix.shape[1]
-    block_rows = lax.all_gather(hidden_state, "tp", axis=0, tiled=True)
+    copies = jnp.concatenate([hidden_state] * lax.axis_size("tp"), axis=0)
+    block_rows = lax.all_to_all(copies, "tp", 0, 0, tiled=True)
     row_count = block_rows.shape[0]
     position = offset + jnp.arange(row_count, dtype=jnp.int32)
     query_row_block = jnp.dot(block_rows, query_weight, preferred_element_type=jnp.float32)

time: 189 us -> 220 us (1.16)
  the two profiles are of different devices: /device:TPU:128 before, /device:TPU:1 now
where the time goes in v1:
time: 220 us; the launch traced here: 219 us
  blocking collectives  106 us (48%)
  waiting for transfers between devices  43.5 us (20%)
  other arithmetic  20.7 us (9%)
  matrix products  20.7 us (9%)
  starting transfers between devices  17.3 us (8%)
  local copies, waits for them, and re-layouts  10.2 us (5%)
    all_to_all x1, blocking collectives, summed_on_arrival(): blocks = lax.all_to_all(in_blocks(x, dim, peers), axis, 0, 0, tiled=True)  44 us
    psum x2, blocking collectives, one_axis_at_a_time(): return functools.reduce(lax.psum, axes, x)  39.6 us
    all_to_all x1, waiting for transfers between devices, shards(): block_rows = lax.all_to_all(copies, 'tp', 0, 0, tiled=True)  34.5 us
    all_gather x1, blocking collectives, side_by_side(): out, at, outs = (lax.all_gather(both, axis, axis=dim, tiled=True), 0, [])  22.7 us
    all_to_all x1, waiting for transfers between devices, sent_to_all(): lax.all_to_all(jnp.broadcast_to(x[None], (peers, *x.shape)), axis, 0, 0,...  9.01 us
    all_to_all x1, starting transfers between devices, sent_to_all(): lax.all_to_all(jnp.broadcast_to(x[None], (peers, *x.shape)), axis, 0, 0,...  7.64 us
    unnamed x30, local copies, waits for them, and re-layouts  5.73 us
    unnamed x8, other arithmetic  5.32 us
  transfers between devices with their start and end apart: 4, of which 2 were waited for; matrix products, arithmetic and copies ran while one was open for 11% of the time, Pallas kernels for 0%

profile of v1, /device:TPU:1, one launch (start us, length us, event | category | flops | bytes accessed | tf_op | source)
XLA Modules:
  0.0 219.0 jit_solution(5329146499534180506)
XLA Ops:
  0.0 1.3 fusion.20
  4.5 30.7 %all-reduce = (f32[1,256]{1,0:T(1,128)S(1)}, f32[2,256]{1,0:T(2,128)S(1)}, f32[2,256]{1,0:T(2,128)S(1)}) all-reduce(f32[1,256]{1,0:T(1,128)S(1)} %fusion.59, f32[2,256]{1,0:T(2,128)S(1)} %fusion.71, f32[2,256]{1,0:T(2,128)S(1)} %fusion.70), channel_id=1, replica_groups=mesh['sp_0'=16,'sp_1'=4,'tp'=8] {'sp_0'}, use_global_device_ids=true, to_apply=%region_4.5 | all-reduce | flops 1280 | bytes 10240 | tf_op jit(solution)/shard_map/psum | solution.py:20
  35.3 8.8 %all-reduce.1 = (f32[1,256]{1,0:T(1,128)S(1)}, f32[2,256]{1,0:T(2,128)S(1)}, f32[2,256]{1,0:T(2,128)S(1)}) all-reduce(f32[1,256]{1,0:T(1,128)S(1)} %get-tuple-element.5, f32[2,256]{1,0:T(2,128)S(1)} %get-tuple-element.6, f32[2,256]{1,0:T(2,128)S(1)} %get-tuple-element.7), channel_id=1, replica_groups=mesh['sp_0'=16,'sp_1'=4,'tp'=8] {'sp_1'}, use_global_device_ids=true, to_apply=%region_5.6 | all-reduce | flops 1280 | bytes 10240 | tf_op jit(solution)/shard_map/psum | solution.py:20
  44.1 22.7 %all_gather.3 = f32[5,2048]{1,0:T(8,128)S(1)} all-gather(f32[5,256]{1,0:T(8,128)S(1)} %pad_maximum_fusion.12), channel_id=1, replica_groups=mesh['sp_0'=16,'sp_1'=4,'tp'=8] {'tp'}, dimensions={1}, use_global_device_ids=true | all-gather | bytes 46080 | tf_op jit(solution)/shard_map/all_gather | solution.py:25
  68.1 1.2 constant_dynamic-update-slice_fusion.6
  72.4 1.7 copy-done.2
  74.1 4.6 %all-to-all-start = ((bf16[8,96,2048]{2,1,0:T(8,128)(2,1)}), bf16[8,96,2048]{2,1,0:T(8,128)(2,1)}, u32[]{:S(2)}, u32[]{:S(2)}) async-start(bf16[8,96,2048]{2,1,0:T(8,128)(2,1)} %bitcast.156), calls=%async_computation | async-start | bytes 6291456 | tf_op jit(solution)/shard_map/all_to_all | solution.py:134
  80.4 1.4 fusion.18
  81.8 34.5 %all-to-all-done = bf16[8,96,2048]{2,1,0:T(8,128)(2,1)} async-done(((bf16[8,96,2048]{2,1,0:T(8,128)(2,1)}), bf16[8,96,2048]{2,1,0:T(8,128)(2,1)}, u32[]{:S(2)}, u32[]{:S(2)}) %all-to-all-start) | async-done | bytes 3145760 | tf_op jit(solution)/shard_map/all_to_all | solution.py:134
  117.1 7.6 %all-to-all-start.1 = ((bf16[64,16,256]{2,1,0:T(8,128)(2,1)}), bf16[64,16,256]{2,1,0:T(8,128)(2,1)S(1)}, u32[]{:S(2)}, u32[]{:S(2)}) async-start(bf16[64,16,256]{2,1,0:T(8,128)(2,1)} %broadcast_in_dim.12), calls=%async_computation.1 | async-start | bytes 1048576 | tf_op jit(solution)/shard_map/all_to_all | solution.py:47
  124.8 1.4 fusion.39
  127.2 1.5 copy.32
  128.7 2.9 %fusion.72 = f32[768,2,2,2,32]{0,4,3,2,1:T(8,128)S(1)} fusion(bf16[768,2048,1,1,1]{1,0,4,3,2:T(8,128)(2,1)} %bitcast.30, bf16[2,2,2,32,2048]{4,3,2,1,0:T(8,128)(2,1)S(1)} %bitcast.162), kind=kOutput, calls=%fused_computation.135 | convolution fusion | flops 805306368 | bytes 4980736 | tf_op jit(solution)/shard_map/dot_general | solution.py:137
  132.6 3.2 %convolution_bitcast_fusion.1 = f32[768,1,2,2,32]{0,4,3,2,1:T(8,128)S(1)} fusion(bf16[768,2048,1,1]{1,0,3,2:T(8,128)(2,1)} %bitcast.11, bf16[2,2,32,2048]{3,2,1,0:T(8,128)(2,1)} %bitcast.181), kind=kOutput, calls=%fused_computation.19 | convolution fusion | flops 402653184 | bytes 4063232 | tf_op jit(solution)/shard_map/dot_general | solution.py:139
  136.7 3.0 %convolution_convert_fusion.1 = bf16[768,128]{1,0:T(8,128)(2,1)S(1)} fusion(bf16[768,2048]{1,0:T(8,128)(2,1)} %bitcast.9, bf16[2048,128]{1,0:T(8,128)(2,1)} %param.23), kind=kOutput, calls=%fused_computation.28 | convolution fusion | flops 402751488 | bytes 3866624 | tf_op jit(solution)/shard_map/dot_general | solution.py:141
  140.4 3.6 %collective-permute-start = (bf16[128,256]{1,0:T(8,128)(2,1)}, bf16[128,256]{1,0:T(8,128)(2,1)}, u32[]{:S(2)}, u32[]{:S(2)}) collective-permute-start(bf16[128,256]{1,0:T(8,128)(2,1)} %get-tuple-element.21), channel_id=1, source_target_pairs={{0,8},{8,16},{16,24},{24,32},{32,40},{40,48},{48,56},{56,64},{64,7... | collective-permute-start | bytes 196616 | tf_op jit(solution)/shard_map/ppermute | solution.py:37
  143.9 1.5 collective-permute-start.1
  145.4 9.0 %all-to-all-done.1 = bf16[64,16,256]{2,1,0:T(8,128)(2,1)S(1)} async-done(((bf16[64,16,256]{2,1,0:T(8,128)(2,1)}), bf16[64,16,256]{2,1,0:T(8,128)(2,1)S(1)}, u32[]{:S(2)}, u32[]{:S(2)}) %all-to-all-start.1) | async-done | bytes 524320 | tf_op jit(solution)/shard_map/all_to_all | solution.py:47
  154.4 3.6 %bitcast_reduce_fusion = (f32[6,2,128]{2,1,0:T(2,128)S(1)}, f32[1024,6,128,2]{2,0,3,1:T(8,128)}) fusion(bf16[6,128,2,128]{3,1,2,0:T(8,128)(2,1)S(1)} %copy.33, bf16[1024,256]{1,0:T(8,128)(2,1)S(1)} %bitcast.160), kind=kOutput, calls=%fused_computation.1 | convolution fusion | flops 405797376 | bytes 6952960 | tf_op jit(solution)/shard_map/nqhgd,chd->nhgqc/dot_general | solution.py:194
  160.0 1.6 pad_maximum_fusion.6
  162.0 1.6 fusion.6
  163.7 3.9 %fusion.1 = f32[6,2,128]{2,1,0:T(2,128)S(1)} fusion(f32[1024,6,128,2]{2,0,3,1:T(8,128)} %get-tuple-element.41, f32[6,2,128]{2,1,0:T(2,128)S(1)} %maximum_maximum_fusion), kind=kLoop, calls=%fused_computation.5 | loop fusion | flops 4717056 | bytes 6303744 | tf_op jit(solution)/shard_map/reduce_sum | solution.py:211
  170.6 1.5 fusion.13
  173.5 44.0 %all_to_all.22 = bf16[8,96,2048]{2,1,0:T(8,128)(2,1)S(1)} all-to-all(bf16[8,96,2048]{2,1,0:T(8,128)(2,1)S(1)} %bitcast.155), channel_id=1, replica_groups=mesh['sp_0'=16,'sp_1'=4,'tp'=8] {'tp'}, dimensions={0} | all-to-all | bytes 6291456 | tf_op jit(solution)/shard_map/all_to_all | solution.py:68
  (79 shorter events, 21.7 us)
Async XLA Ops:
  0.0 172.5 %copy-start = (bf16[256,2048]{1,0:T(8,128)(2,1)S(1)}, bf16[256,2048]{1,0:T(8,128)(2,1)}, u32[]{:S(2)}) copy-start(bf16[256,2048]{1,0:T(8,128)(2,1)} %param.25) | copy-start | bytes 3145732
  0.0 70.6 %copy-start.1 = (bf16[96,2048]{1,0:T(8,128)(2,1)S(1)}, bf16[96,2048]{1,0:T(8,128)(2,1)}, u32[]{:S(2)}) copy-start(bf16[96,2048]{1,0:T(8,128)(2,1)} %param.13) | copy-start | bytes 1179652
  0.0 71.5 %copy-start.4 = (f32[2048]{0:T(1024)S(1)}, f32[2048]{0:T(1024)}, u32[]{:S(2)}) copy-start(f32[2048]{0:T(1024)} %param.17) | copy-start | bytes 24580
  72.4 1.7 copy-start.2
  74.1 4.7 %copy-start.6 = (bf16[16,2048]{1,0:T(8,128)(2,1)S(1)}, bf16[16,2048]{1,0:T(8,128)(2,1)}, u32[]{:S(2)}) copy-start(bf16[16,2048]{1,0:T(8,128)(2,1)} %param.16) | copy-start | bytes 196612
  74.1 4.8 %copy-start.7 = (bf16[2048,128]{1,0:T(8,128)(2,1)S(1)}, bf16[2048,128]{1,0:T(8,128)(2,1)}, u32[]{:S(2)}) copy-start(bf16[2048,128]{1,0:T(8,128)(2,1)} %param.23) | copy-start | bytes 1572868
  74.1 5.1 %copy-start.3 = (bf16[2048,128]{1,0:T(8,128)(2,1)S(1)}, bf16[2048,128]{1,0:T(8,128)(2,1)}, u32[]{:S(2)}) copy-start(bf16[2048,128]{1,0:T(8,128)(2,1)} %param.22) | copy-start | bytes 1572868
  74.1 42.2 %all-to-all-start = ((bf16[8,96,2048]{2,1,0:T(8,128)(2,1)}), bf16[8,96,2048]{2,1,0:T(8,128)(2,1)}, u32[]{:S(2)}, u32[]{:S(2)}) async-start(bf16[8,96,2048]{2,1,0:T(8,128)(2,1)} %bitcast.156), calls=%async_computation | async-start | bytes 6291456 | tf_op jit(solution)/shard_map/all_to_all | solution.py:134
  117.1 37.3 %all-to-all-start.1 = ((bf16[64,16,256]{2,1,0:T(8,128)(2,1)}), bf16[64,16,256]{2,1,0:T(8,128)(2,1)S(1)}, u32[]{:S(2)}, u32[]{:S(2)}) async-start(bf16[64,16,256]{2,1,0:T(8,128)(2,1)} %broadcast_in_dim.12), calls=%async_computation.1 | async-start | bytes 1048576 | tf_op jit(solution)/shard_map/all_to_all | solution.py:47
  128.6 3.0 %copy-start.5 = (f32[768,2,32]{0,2,1:T(8,128)S(1)}, f32[768,2,32]{0,2,1:T(8,128)}, u32[]{:S(2)}) copy-start(f32[768,2,32]{0,2,1:T(8,128)} %get-tuple-element.24) | copy-start | bytes 589828
  132.6 3.2 %copy-start.8 = (f32[768,1,1,1,32]{0,4,3,2,1:T(8,128)S(1)}, f32[768,1,1,1,32]{0,4,3,2,1:T(8,128)}, u32[]{:S(2)}) copy-start(f32[768,1,1,1,32]{0,4,3,2,1:T(8,128)} %get-tuple-element.30) | copy-start | bytes 294916
  132.6 3.2 %copy-start.9 = (f32[768,1,1,1,32]{0,4,3,2,1:T(8,128)S(1)}, f32[768,1,1,1,32]{0,4,3,2,1:T(8,128)}, u32[]{:S(2)}) copy-start(f32[768,1,1,1,32]{0,4,3,2,1:T(8,128)} %get-tuple-element.37) | copy-start | bytes 294916
  140.4 19.6 %collective-permute-start = (bf16[128,256]{1,0:T(8,128)(2,1)}, bf16[128,256]{1,0:T(8,128)(2,1)}, u32[]{:S(2)}, u32[]{:S(2)}) collective-permute-start(bf16[128,256]{1,0:T(8,128)(2,1)} %get-tuple-element.21), channel_id=1, source_target_pairs={{0,8},{8,16},{16,24},{24,32},{32,40},{40,48},{48,56},{56,64},{64,7... | collective-permute-start | bytes 196616 | tf_op jit(solution)/shard_map/ppermute | solution.py:37
  143.9 16.0 %collective-permute-start.1 = (bf16[128,256]{1,0:T(8,128)(2,1)}, bf16[128,256]{1,0:T(8,128)(2,1)}, u32[]{:S(2)}, u32[]{:S(2)}) collective-permute-start(bf16[128,256]{1,0:T(8,128)(2,1)} %get-tuple-element.22), channel_id=1, source_target_pairs={{8,0},{16,8},{24,16},{32,24},{40,32},{48,40},{56,48},{64,56},{72,6... | collective-permute-start | bytes 196616 | tf_op jit(solution)/shard_map/ppermute | solution.py:40
  160.0 3.6 %copy-start.11 = (f32[2]{0:T(128)S(1)}, f32[2]{0:T(128)}, u32[]{:S(2)}) copy-start(f32[2]{0:T(128)} %param.24) | copy-start | bytes 28
  163.7 4.5 %copy-start.10 = (bf16[6,128,1,128]{1,3,0,2:T(8,128)(2,1)S(1)}, bf16[6,128,1,128]{1,3,0,2:T(8,128)(2,1)}, u32[]{:S(2)}) copy-start(bf16[6,128,1,128]{1,3,0,2:T(8,128)(2,1)} %copy.29) | copy-start | bytes 589828
  167.6 2.2 slice-start
  168.2 2.4 %slice-start.1 = ((s8[6291456]{0:T(1024)(128)(4,1)}), s8[2097152]{0:T(1024)(128)(4,1)S(1)}, s32[]{:S(2)}) async-start(s8[6291456]{0:T(1024)(128)(4,1)} %bitcast.153), calls=%async_computation.4 | async-start | bytes 4194304
